TPU v7x, 32 devices: a whole 2x2x4 slice. The times are simulated.
32 devices in a mesh: ep: 16 (over z, y, x), tp: 2 (over core).
Axes of the slice: x: 2, y: 2, z: 4, core: 2. Of those that a mesh axis runs over, the one named last changes fastest.
Arguments:
- tokens: bfloat16 [64, 4096], P('ep'), may hold values from -6 to 6
- memory: float32 [64, 8, 256, 512], P('ep', 'tp'), may hold values from -6 to 6
- normalizer: float32 [64, 8, 256], P('ep', 'tp'), may hold values from -6 to 6
- stabilizer: float32 [64, 8], P('ep', 'tp'), may hold values from -4 to 4
- norm_gain: float32 [4096], replicated, may hold values from 0.1 to 1.9
- w_query: bfloat16 [4096, 8, 256], P(None, 'tp', 'ep'), may hold values from -0.09375 to 0.09375
- w_key: bfloat16 [4096, 8, 256], P(None, 'tp', 'ep'), may hold values from -0.09375 to 0.09375
- w_value: bfloat16 [4096, 8, 512], P(None, 'tp', 'ep'), may hold values from -0.09375 to 0.09375
- w_outgate: bfloat16 [4096, 8, 512], P(None, 'tp', 'ep'), may hold values from -0.09375 to 0.09375
- w_input: bfloat16 [4096, 8], P(None, 'tp'), may hold values from -0.09375 to 0.09375
- w_forget: bfloat16 [4096, 8], P(None, 'tp'), may hold values from -0.09375 to 0.09375
- forget_bias: float32 [8], P('tp'), may hold values from 0 to 4
- w_out: bfloat16 [4096, 4096], P('tp', 'ep'), may hold values from -0.09375 to 0.09375
- ffn_gain: float32 [4096], replicated, may hold values from 0.1 to 1.9
- w_gate: bfloat16 [16, 4096, 512], P('ep', None, 'tp'), may hold values from -0.09375 to 0.09375
- w_up: bfloat16 [16, 4096, 512], P('ep', None, 'tp'), may hold values from -0.09375 to 0.09375
- w_down: bfloat16 [16, 512, 4096], P('ep', 'tp'), may hold values from -0.25 to 0.25
- expert_ids: int32 [64, 2], P('ep'), may hold values from 0 to 15, as said below
- route_weights: float32 [64, 2], P('ep'), may hold values from 0.1 to 1
Outputs:
- out: bfloat16 [64, 4096], P('ep')
- memory_next: float32 [64, 8, 256, 512], P('ep', 'tp')
- normalizer_next: float32 [64, 8, 256], P('ep', 'tp')
- stabilizer_next: float32 [64, 8], P('ep', 'tp')
Inputs may be any that keep to these rules, and one draw needn't show every extreme that they name: `expert_ids`: the 2 experts of a token differ and lie in one group of 8 consecutive experts. Beyond that, any choice is allowed: for instance, all 4 tokens of one index of ep may name the same expert.
All inputs are finite; a program needn't handle non-finite values.
Results may differ from a plain program's by a relative error of at most 0.013.
Values may be sent and summed in bfloat16 or wider, within the bound.
No kernel may reach another device: no remote copies, remote signals or barrier semaphores. Data moves between devices by JAX's collectives and lax.ppermute only.
A program may use at most 128 MiB of HBM per device.

v0:
```python
import jax
import jax.numpy as jnp
from jax import lax
from jax.sharding import PartitionSpec as P


def rms_scale(values, gain):
    return values * lax.rsqrt(jnp.mean(values * values, axis=-1, keepdims=True) + 1e-06) * gain


def product(left, right):
    return jnp.dot(left, right, preferred_element_type=jnp.float32)


def rounded_term(values):
    return lax.optimization_barrier(values.astype(jnp.bfloat16)).astype(jnp.float32)


def body(
    tokens,
    memory,
    normalizer,
    stabilizer,
    norm_gain,
    w_query,
    w_key,
    w_value,
    w_outgate,
    w_input,
    w_forget,
    forget_bias,
    w_out,
    ffn_gain,
    w_gate,
    w_up,
    w_down,
    expert_ids,
    route_weights,
):
    seqs, width = tokens.shape
    heads, key_size, value_size = (memory.shape[1], memory.shape[2], memory.shape[3])
    value_width = heads * value_size
    key_piece = w_query.shape[2]
    value_piece = w_value.shape[2]
    query_cols = w_query.reshape(width, heads * key_piece)
    key_cols = w_key.reshape(width, heads * key_piece)
    value_cols = w_value.reshape(width, heads * value_piece)
    outgate_cols = w_outgate.reshape(width, heads * value_piece)
    normed = rms_scale(tokens.astype(jnp.float32), norm_gain).astype(jnp.bfloat16)
    piece = lax.all_gather(normed, "ep", axis=0, tiled=True)
    projected = jnp.concatenate(
        [
            product(piece, query_cols),
            product(piece, key_cols),
            product(piece, value_cols),
            product(piece, outgate_cols),
        ],
        axis=1,
    ).astype(jnp.bfloat16)
    all_rows = projected.shape[0]
    narrow = heads * key_piece
    broad = heads * value_piece
    query_part = projected[:, :narrow].reshape(all_rows, heads, key_piece)
    key_part = projected[:, narrow : 2 * narrow].reshape(all_rows, heads, key_piece)
    value_part = projected[:, 2 * narrow : 2 * narrow + broad].reshape(all_rows, heads, value_piece)
    outgate_part = projected[:, 2 * narrow + broad :].reshape(all_rows, heads, value_piece)
    query, key, value, outgate = (
        lax.all_to_all(query_part, "ep", split_axis=0, concat_axis=2, tiled=True),
        lax.all_to_all(key_part, "ep", split_axis=0, concat_axis=2, tiled=True),
        lax.all_to_all(value_part, "ep", split_axis=0, concat_axis=2, tiled=True),
        lax.all_to_all(outgate_part, "ep", split_axis=0, concat_axis=2, tiled=True),
    )
    in_pre = product(normed, w_input)
    log_forget = jax.nn.log_sigmoid(product(normed, w_forget) + forget_bias)
    scaled = query.astype(jnp.float32) * key_size ** (-0.5)
    key_heads = key.astype(jnp.float32)
    value_heads = value.astype(jnp.float32)
    stab_next = jnp.maximum(log_forget + stabilizer, in_pre)
    decay = jnp.exp(log_forget + stabilizer - stab_next)
    inweight = jnp.exp(in_pre - stab_next)
    memory_next = decay[:, :, None, None] * memory + inweight[:, :, None, None] * (
        key_heads[:, :, :, None] * value_heads[:, :, None, :]
    )
    normalizer_next = decay[:, :, None] * normalizer + inweight[:, :, None] * key_heads
    numerator = jnp.einsum("shd,shde->she", scaled, memory_next, precision=lax.Precision.HIGHEST)
    denominator = jnp.sum(scaled * normalizer_next, axis=-1)
    hidden = numerator / jnp.maximum(jnp.abs(denominator), jnp.exp(-stab_next))[:, :, None]
    hidden = (
        hidden.reshape(seqs, value_width)
        * jax.nn.sigmoid(outgate.reshape(seqs, value_width).astype(jnp.float32))
    ).astype(jnp.bfloat16)
    partial_value = product(lax.all_gather(hidden, "ep", axis=0, tiled=True), w_out)
    summed = lax.psum(rounded_term(partial_value).astype(jnp.bfloat16), "tp")
    mixed = lax.all_to_all(summed, "ep", split_axis=0, concat_axis=1, tiled=True)
    resid = tokens.astype(jnp.float32) + mixed.astype(jnp.float32)
    ffn_in = rms_scale(resid, ffn_gain).astype(jnp.bfloat16)
    gate_local, up_local, down_local = (w_gate[0], w_up[0], w_down[0])
    n_experts = lax.axis_size("ep") * w_gate.shape[0]
    piece = lax.all_gather(ffn_in, "ep", axis=0, tiled=True)
    gate_part = product(piece, gate_local)
    up_part = product(piece, up_local)
    act = (jax.nn.silu(gate_part) * up_part).astype(jnp.bfloat16)
    expert_terms = rounded_term(product(act, down_local))
    labels = jnp.arange(n_experts, dtype=jnp.int32)
    route_dense = jnp.sum(
        jnp.where(expert_ids[:, :, None] == labels[None, None, :], route_weights[:, :, None], 0.0),
        axis=1,
    )
    my_weight = lax.all_to_all(route_dense, "ep", split_axis=1, concat_axis=0, tiled=True)
    contrib = expert_terms * my_weight
    n_ep = lax.axis_size("ep")
    n_tp = lax.axis_size("tp")
    arranged = jnp.swapaxes(contrib.reshape(n_ep, seqs, n_tp, width // n_tp), 1, 2)
    arranged = arranged.reshape(n_ep * n_tp * seqs, width // n_tp)
    mine = lax.psum_scatter(arranged, ("ep", "tp"), scatter_dimension=0, tiled=True)
    ffn_out = lax.all_gather(mine.astype(jnp.bfloat16), "tp", axis=1, tiled=True).astype(mine.dtype)
    out = (resid + ffn_out).astype(jnp.bfloat16)
    return (out, memory_next, normalizer_next, stab_next)


def solution(mesh):
    return jax.shard_map(
        body,
        mesh=mesh,
        in_specs=(
            P("ep", None),
            P("ep", "tp", None, None),
            P("ep", "tp", None),
            P("ep", "tp"),
            P(),
            P(None, "tp", "ep"),
            P(None, "tp", "ep"),
            P(None, "tp", "ep"),
            P(None, "tp", "ep"),
            P(None, "tp"),
            P(None, "tp"),
            P("tp"),
            P("tp", "ep"),
            P(),
            P("ep", None, "tp"),
            P("ep", None, "tp"),
            P("ep", "tp", None),
            P("ep", None),
            P("ep", None),
        ),
        out_specs=(P("ep", None), P("ep", "tp", None, None), P("ep", "tp", None), P("ep", "tp")),
        check_vma=False,
    )
```

profile of v0, /device:TPU:0, one launch (start us, length us, event | category | flops | bytes accessed | tf_op | source)
XLA Modules:
  0.0 274.0 jit_solution(16929384175384432204)
XLA Ops:
  0.7 1.1 fusion.14
  1.7 0.9 fusion.49
  2.6 45.3 %all-gather = bf16[16,4,4096]{2,1,0:T(4,128)(2,1)S(1)} all-gather(bf16[1,4,4096]{2,1,0:T(4,128)(2,1)S(1)} %fusion.49), channel_id=1, replica_groups=mesh['ep'=16,'tp'=2] {'ep'}, dimensions={0}, use_global_device_ids=true | all-gather | bytes 557056 | tf_op jit(solution)/shard_map/all_gather | solution.py:50
  47.9 0.1 reshape.133
  48.0 1.3 convolution_convert_fusion.4
  49.5 0.1 copy.119
  49.6 0.7 reshape.153
  50.3 3.5 %all-to-all-start.1 = ((bf16[16,2,128]{2,1,0:T(2,128)(2,1)}), bf16[16,2,128]{2,1,0:T(2,128)(2,1)S(1)}, u32[]{:S(2)}, u32[]{:S(2)}) async-start(bf16[16,2,128]{2,1,0:T(2,128)(2,1)} %reshape.153), calls=%async_computation.1 | async-start | bytes 16384 | tf_op jit(solution)/shard_map/all_to_all | solution.py:69
  53.8 0.8 fusion.16
  54.6 0.9 fusion.29
  55.5 0.9 subtract_exponential_fusion.1
  56.5 1.3 convolution_convert_fusion.5
  57.9 1.7 convolution_convert_fusion.3
  59.6 1.7 convolution_convert_fusion.2
  61.3 0.8 select_reduce_fusion
  62.2 0.1 copy.114
  62.3 0.7 reshape.149
  63.0 0.1 copy.122
  63.1 0.1 copy.123
  63.2 0.7 reshape.151
  63.9 0.1 copy.126
  64.1 0.1 copy.127
  64.2 0.7 reshape.155
  64.9 0.7 copy.131
  65.6 6.9 %all-to-all-start = ((bf16[16,2,128]{2,1,0:T(2,128)(2,1)}), bf16[16,2,128]{2,1,0:T(2,128)(2,1)S(1)}, u32[]{:S(2)}, u32[]{:S(2)}) async-start(bf16[16,2,128]{2,1,0:T(2,128)(2,1)} %reshape.149), calls=%async_computation | async-start | bytes 16384 | tf_op jit(solution)/shard_map/all_to_all | solution.py:68
  72.5 0.1 reshape.154
  72.6 0.1 reshape.120
  72.7 7.0 %all-to-all-done = bf16[16,2,128]{2,1,0:T(2,128)(2,1)S(1)} async-done(((bf16[16,2,128]{2,1,0:T(2,128)(2,1)}), bf16[16,2,128]{2,1,0:T(2,128)(2,1)S(1)}, u32[]{:S(2)}, u32[]{:S(2)}) %all-to-all-start) | async-done | bytes 8224 | tf_op jit(solution)/shard_map/all_to_all | solution.py:68
  79.7 3.5 %all-to-all-start.2 = ((bf16[16,2,256]{2,1,0:T(2,128)(2,1)}), bf16[16,2,256]{2,1,0:T(2,128)(2,1)S(1)}, u32[]{:S(2)}, u32[]{:S(2)}) async-start(bf16[16,2,256]{2,1,0:T(2,128)(2,1)} %reshape.151), calls=%async_computation.2 | async-start | bytes 32768 | tf_op jit(solution)/shard_map/all_to_all | solution.py:70
  83.2 0.1 reshape.150
  83.4 0.1 copy.116
  83.5 0.1 mul.130
  83.6 0.7 multiply_reduce_fusion.1
  84.3 0.1 reshape.141
  84.5 6.1 %all-to-all-done.2 = bf16[16,2,256]{2,1,0:T(2,128)(2,1)S(1)} async-done(((bf16[16,2,256]{2,1,0:T(2,128)(2,1)}), bf16[16,2,256]{2,1,0:T(2,128)(2,1)S(1)}, u32[]{:S(2)}, u32[]{:S(2)}) %all-to-all-start.2) | async-done | bytes 16416 | tf_op jit(solution)/shard_map/all_to_all | solution.py:70
  90.6 3.5 %all-to-all-start.3 = ((bf16[16,2,256]{2,1,0:T(2,128)(2,1)}), bf16[16,2,256]{2,1,0:T(2,128)(2,1)S(1)}, u32[]{:S(2)}, u32[]{:S(2)}) async-start(bf16[16,2,256]{2,1,0:T(2,128)(2,1)} %reshape.155), calls=%async_computation.3 | async-start | bytes 32768 | tf_op jit(solution)/shard_map/all_to_all | solution.py:71
  94.0 0.1 reshape.152
  94.2 0.1 reshape.121
  94.3 4.2 %multiply_add_fusion = f32[4,4,256,512]{3,2,1,0:T(8,128)S(1)} fusion(f32[4,4,256,512]{3,2,1,0:T(8,128)} %param.20, f32[4,4,512]{2,1,0:T(4,128)S(1)} %reshape.121, f32[4,4,256]{2,1,0:T(4,128)S(1)} %reshape.120, f32[4,4]{1,0:T(4,128)S(1)} %subtract_exponential_fusion, f32[4,4]{1,0:T(4,128)S(1)} %get-tuple-element.6), kind=kLoop, calls=%fused_computation | loop fusion | flops 8388608 | bytes 16826496 | tf_op jit(solution)/shard_map/add | solution.py:81
  98.5 3.4 %copy-done.1 = f32[4,4,256,512]{3,2,1,0:T(8,128)} copy-done((f32[4,4,256,512]{3,2,1,0:T(8,128)}, f32[4,4,256,512]{3,2,1,0:T(8,128)S(1)}, u32[]{:S(2)}) %copy-start.1) | copy-done | bytes 8388632
  101.9 4.0 %fusion.30 = f32[4,4,1,512]{3,2,1,0:T(1,128)S(1)} fusion(f32[4,4,256,1]{2,3,1,0:T(1,128)S(1)} %reshape.141, f32[4,4,256,512]{3,2,1,0:T(8,128)S(1)} %multiply_add_fusion), kind=kOutput, calls=%fused_computation.57 | convolution fusion | flops 25165824 | bytes 8437760 | tf_op jit(solution)/shard_map/shd,shde->she/dot_general | solution.py:85
  106.1 6.9 %all-to-all-start.5 = ((f32[4,16,1]{0,2,1:T(1,128)}), f32[4,16,1]{0,2,1:T(1,128)S(1)}, u32[]{:S(2)}, u32[]{:S(2)}) async-start(f32[4,16,1]{0,2,1:T(1,128)} %copy.131), calls=%async_computation.5 | async-start | bytes 16384 | tf_op jit(solution)/shard_map/all_to_all | solution.py:109
  113.0 0.1 reshape.156
  113.1 0.1 copy.128
  113.2 0.1 copy.129
  113.3 0.1 reshape.124
  113.5 42.4 %all-gather.1 = bf16[16,4,2048]{2,1,0:T(4,128)(2,1)S(1)} all-gather(bf16[1,4,2048]{2,1,0:T(4,128)(2,1)S(1)} %fusion.25), channel_id=1, replica_groups=mesh['ep'=16,'tp'=2] {'ep'}, dimensions={0}, use_global_device_ids=true | all-gather | bytes 278528 | tf_op jit(solution)/shard_map/all_gather | solution.py:92
  155.8 0.8 reshape.135
  156.6 1.2 convolution_convert_fusion.1
  157.9 4.0 %psum.7 = bf16[16,4,256]{2,1,0:T(4,128)(2,1)} all-reduce(bf16[16,4,256]{2,1,0:T(4,128)(2,1)S(1)} %all_to_all.24), channel_id=1, replica_groups=mesh['ep'=16,'tp'=2] {'tp'}, use_global_device_ids=true, to_apply=%region_2.3 | all-reduce | flops 16384 | bytes 65536 | tf_op jit(solution)/shard_map/psum | solution.py:93
  161.9 3.5 %all-to-all-start.4 = ((bf16[16,4,256]{2,1,0:T(4,128)(2,1)}), bf16[16,4,256]{2,1,0:T(4,128)(2,1)S(1)}, u32[]{:S(2)}, u32[]{:S(2)}) async-start(bf16[16,4,256]{2,1,0:T(4,128)(2,1)} %psum.7), calls=%async_computation.4 | async-start | bytes 65536 | tf_op jit(solution)/shard_map/all_to_all | solution.py:94
  165.5 7.3 %all-to-all-done.4 = bf16[16,4,256]{2,1,0:T(4,128)(2,1)S(1)} async-done(((bf16[16,4,256]{2,1,0:T(4,128)(2,1)}), bf16[16,4,256]{2,1,0:T(4,128)(2,1)S(1)}, u32[]{:S(2)}, u32[]{:S(2)}) %all-to-all-start.4) | async-done | bytes 32800 | tf_op jit(solution)/shard_map/all_to_all | solution.py:94
  172.8 0.1 multiply_reduce_fusion
  173.0 39.4 %all-gather.2 = bf16[16,4,4096]{2,1,0:T(4,128)(2,1)S(1)} all-gather(bf16[1,4,4096]{2,1,0:T(4,128)(2,1)S(1)} %fusion.22), channel_id=1, replica_groups=mesh['ep'=16,'tp'=2] {'ep'}, dimensions={0}, use_global_device_ids=true | all-gather | bytes 557056 | tf_op jit(solution)/shard_map/all_gather | solution.py:99
  212.4 0.1 reshape.137
  212.5 2.0 fusion.3
  214.6 3.8 %convolution_convert_fusion = bf16[64,4096]{1,0:T(8,128)(2,1)} fusion(bf16[1,256,4096]{2,1,0:T(8,128)(2,1)S(1)} %copy-done, bf16[64,4096]{1,0:T(8,128)(2,1)S(1)} %reshape.137, bf16[1,4096,256]{2,1,0:T(8,128)(2,1)} %param.34, f32[64,256]{1,0:T(8,128)S(1)} %fusion.3), kind=kOutput, calls=%fused_computation.1 | convolution fusion | flops 268795904 | bytes 5308416 | tf_op jit(solution)/shard_map/dot_general | solution.py:12
  218.4 1.2 convert_multiply_fusion
  219.6 1.9 reshape.118
  221.4 1.9 copy.132
  223.4 1.3 reshape.119
  224.7 46.8 %all-reduce.2 = bf16[128,2048]{1,0:T(8,128)(2,1)S(1)} all-reduce(f32[128,2048]{1,0:T(8,128)} %reshape.119), channel_id=2, replica_groups=mesh['ep'=16,'tp'=2] {'ep','tp'}, use_global_device_ids=true, to_apply=%region_5.6.clone | all-reduce | flops 262144 | bytes 1572864
  271.5 1.8 all_gather.15
  273.4 0.6 add_convert_fusion
  (42 shorter events, 0.8 us)
Async XLA Ops:
  0.6 214.0 %copy-start = (bf16[1,256,4096]{2,1,0:T(8,128)(2,1)S(1)}, bf16[1,256,4096]{2,1,0:T(8,128)(2,1)}, u32[]{:S(2)}) copy-start(bf16[1,256,4096]{2,1,0:T(8,128)(2,1)} %param.35) | copy-start | bytes 6291460
  0.6 83.0 %copy-start.5 = (f32[4,4,256]{2,1,0:T(4,128)S(1)}, f32[4,4,256]{2,1,0:T(4,128)}, u32[]{:S(2)}) copy-start(f32[4,4,256]{2,1,0:T(4,128)} %param.21) | copy-start | bytes 49156
  50.3 15.3 %all-to-all-start.1 = ((bf16[16,2,128]{2,1,0:T(2,128)(2,1)}), bf16[16,2,128]{2,1,0:T(2,128)(2,1)S(1)}, u32[]{:S(2)}, u32[]{:S(2)}) async-start(bf16[16,2,128]{2,1,0:T(2,128)(2,1)} %reshape.153), calls=%async_computation.1 | async-start | bytes 16384 | tf_op jit(solution)/shard_map/all_to_all | solution.py:69
  56.5 42.0 %copy-start.6 = (f32[4,4]{1,0:T(4,128)}, f32[4,4]{1,0:T(4,128)S(1)}, u32[]{:S(2)}) copy-start(f32[4,4]{1,0:T(4,128)S(1)} %get-tuple-element.7) | copy-start | bytes 196
  65.6 14.1 %all-to-all-start = ((bf16[16,2,128]{2,1,0:T(2,128)(2,1)}), bf16[16,2,128]{2,1,0:T(2,128)(2,1)S(1)}, u32[]{:S(2)}, u32[]{:S(2)}) async-start(bf16[16,2,128]{2,1,0:T(2,128)(2,1)} %reshape.149), calls=%async_computation | async-start | bytes 16384 | tf_op jit(solution)/shard_map/all_to_all | solution.py:68
  79.7 10.9 %all-to-all-start.2 = ((bf16[16,2,256]{2,1,0:T(2,128)(2,1)}), bf16[16,2,256]{2,1,0:T(2,128)(2,1)S(1)}, u32[]{:S(2)}, u32[]{:S(2)}) async-start(bf16[16,2,256]{2,1,0:T(2,128)(2,1)} %reshape.151), calls=%async_computation.2 | async-start | bytes 32768 | tf_op jit(solution)/shard_map/all_to_all | solution.py:70
  90.6 15.5 %all-to-all-start.3 = ((bf16[16,2,256]{2,1,0:T(2,128)(2,1)}), bf16[16,2,256]{2,1,0:T(2,128)(2,1)S(1)}, u32[]{:S(2)}, u32[]{:S(2)}) async-start(bf16[16,2,256]{2,1,0:T(2,128)(2,1)} %reshape.155), calls=%async_computation.3 | async-start | bytes 32768 | tf_op jit(solution)/shard_map/all_to_all | solution.py:71
  98.5 3.4 %copy-start.1 = (f32[4,4,256,512]{3,2,1,0:T(8,128)}, f32[4,4,256,512]{3,2,1,0:T(8,128)S(1)}, u32[]{:S(2)}) copy-start(f32[4,4,256,512]{3,2,1,0:T(8,128)S(1)} %multiply_add_fusion) | copy-start | bytes 25165828
  101.9 54.7 %copy-start.3 = (bf16[2048,256]{1,0:T(8,128)(2,1)S(1)}, bf16[2048,256]{1,0:T(8,128)(2,1)}, u32[]{:S(2)}) copy-start(bf16[2048,256]{1,0:T(8,128)(2,1)} %param.31) | copy-start | bytes 3145732
  101.9 70.8 %copy-start.2 = (bf16[4,4096]{1,0:T(4,128)(2,1)S(1)}, bf16[4,4096]{1,0:T(4,128)(2,1)}, u32[]{:S(2)}) copy-start(bf16[4,4096]{1,0:T(4,128)(2,1)} %param.19) | copy-start | bytes 98308
  101.9 71.0 %copy-start.4 = (f32[4096]{0:T(1024)S(1)}, f32[4096]{0:T(1024)}, u32[]{:S(2)}) copy-start(f32[4096]{0:T(1024)} %param.32) | copy-start | bytes 49156
  106.1 55.8 %all-to-all-start.5 = ((f32[4,16,1]{0,2,1:T(1,128)}), f32[4,16,1]{0,2,1:T(1,128)S(1)}, u32[]{:S(2)}, u32[]{:S(2)}) async-start(f32[4,16,1]{0,2,1:T(1,128)} %copy.131), calls=%async_computation.5 | async-start | bytes 16384 | tf_op jit(solution)/shard_map/all_to_all | solution.py:109
  161.9 10.9 %all-to-all-start.4 = ((bf16[16,4,256]{2,1,0:T(4,128)(2,1)}), bf16[16,4,256]{2,1,0:T(4,128)(2,1)S(1)}, u32[]{:S(2)}, u32[]{:S(2)}) async-start(bf16[16,4,256]{2,1,0:T(4,128)(2,1)} %psum.7), calls=%async_computation.4 | async-start | bytes 65536 | tf_op jit(solution)/shard_map/all_to_all | solution.py:94
where the time goes:
time: 275 us; the launch traced here: 274 us
  blocking collectives  180 us (65%)
  starting transfers between devices  27.7 us (10%)
  waiting for transfers between devices  20.3 us (7%)
  matrix products  19 us (7%)
  local copies, waits for them, and re-layouts  15.6 us (6%)
  other arithmetic  10.7 us (4%)
    unnamed x1, blocking collectives  46.8 us
    all_gather x1, blocking collectives, body(): piece = lax.all_gather(normed, 'ep', axis=0, tiled=True)  45.3 us
    all_gather x1, blocking collectives, body(): lax.all_gather(hidden, 'ep', axis=0, tiled=True)  42.4 us
    all_gather x1, blocking collectives, body(): piece = lax.all_gather(ffn_in, 'ep', axis=0, tiled=True)  39.4 us
    dot_general x9, matrix products, product(): return jnp.dot(left, right, preferred_element_type=jnp.float32)  15 us
    unnamed x26, local copies, waits for them, and re-layouts  7.67 us
    all_to_all x1, waiting for transfers between devices, body(): lax.all_to_all(summed, 'ep', split_axis=0, concat_axis=1, tiled=True)  7.25 us
    all_to_all x1, waiting for transfers between devices, body(): lax.all_to_all(query_part, 'ep', split_axis=0, concat_axis=2, tiled=True)  6.95 us
  transfers between devices with their start and end apart: 6, of which 3 were waited for; matrix products, arithmetic and copies ran while one was open for 9% of the time, Pallas kernels for 0%

commit v1 on v0

--- a/solution.py
+++ b/solution.py
@@ -96,7 +96,12 @@
     ffn_in = rms_scale(resid, ffn_gain).astype(jnp.bfloat16)
     gate_local, up_local, down_local = (w_gate[0], w_up[0], w_down[0])
     n_experts = lax.axis_size("ep") * w_gate.shape[0]
-    piece = lax.all_gather(ffn_in, "ep", axis=0, tiled=True)
+    ring = [ffn_in]
+    for hop in range(15):
+        ring.append(lax.ppermute(ring[-1], "ep", [(dev, (dev + 1) % 16) for dev in range(16)]))
+    piece = jnp.roll(
+        jnp.concatenate(ring[::-1], axis=0), (lax.axis_index("ep") + 1) * ring[0].shape[0], axis=0
+    )
     gate_part = product(piece, gate_local)
     up_part = product(piece, up_local)
     act = (jax.nn.silu(gate_part) * up_part).astype(jnp.bfloat16)

time: 275 us -> 350 us (1.27)
  waiting for transfers between devices: 20.3 us -> 116 us
  blocking collectives: 180 us -> 151 us
  local copies, waits for them, and re-layouts: 15.6 us -> 25 us
    ppermute x0 -> x15, waiting for transfers between devices: none -> 97.7 us  [body(): lax.ppermute(ring[-1], 'ep', [(dev, (dev + 1) % 16) for dev in range(16)])]
    all_gather x1 -> x0, blocking collectives: 39.4 us -> none  [body(): piece = lax.all_gather(ffn_in, 'ep', axis=0, tiled=True)]
    all_to_all x0 -> x1, blocking collectives: none -> 9.98 us  [body(): lax.all_to_all(summed, 'ep', split_axis=0, concat_axis=1, tiled=True)]
    all_to_all x1 -> x0, waiting for transfers between devices: 7.25 us -> none  [body(): lax.all_to_all(summed, 'ep', split_axis=0, concat_axis=1, tiled=True)]
    concatenate x0 -> x1, local copies, waits for them, and re-layouts: none -> 7.14 us  [body(): jnp.roll(jnp.concatenate(ring[::-1], axis=0), (lax.axis_index('ep') + 1)...]
    all_to_all x1, waiting for transfers between devices: 0.01 us -> 5.12 us  [body(): lax.all_to_all(route_dense, 'ep', split_axis=1, concat_axis=0, tiled=True)]
    unnamed x26 -> x41, local copies, waits for them, and re-layouts: 7.67 us -> 9.98 us
  transfers between devices with their start and end apart: 6 -> 20, of which waited for: 3 -> 17; matrix products, arithmetic and copies ran while one was open for 9% -> 6% of each run, Pallas kernels for 0% -> 0%
where the time goes in v1:
time: 350 us; the launch traced here: 349 us
  blocking collectives  151 us (43%)
  waiting for transfers between devices  116 us (33%)
  starting transfers between devices  27.2 us (8%)
  local copies, waits for them, and re-layouts  25 us (7%)
  matrix products  19.1 us (5%)
  other arithmetic  9.97 us (3%)
    ppermute x15, waiting for transfers between devices, body(): lax.ppermute(ring[-1], 'ep', [(dev, (dev + 1) % 16) for dev in range(16)])  97.7 us
    unnamed x1, blocking collectives  47.6 us
    all_gather x1, blocking collectives, body(): piece = lax.all_gather(normed, 'ep', axis=0, tiled=True)  45.3 us
    all_gather x1, blocking collectives, body(): lax.all_gather(hidden, 'ep', axis=0, tiled=True)  42.3 us
    dot_general x9, matrix products, product(): return jnp.dot(left, right, preferred_element_type=jnp.float32)  15 us
    unnamed x41, local copies, waits for them, and re-layouts  9.98 us
    all_to_all x1, blocking collectives, body(): lax.all_to_all(summed, 'ep', split_axis=0, concat_axis=1, tiled=True)  9.98 us
    concatenate x1, local copies, waits for them, and re-layouts, body(): jnp.roll(jnp.concatenate(ring[::-1], axis=0), (lax.axis_index('ep') + 1)...  7.14 us
  transfers between devices with their start and end apart: 20, of which 17 were waited for; matrix products, arithmetic and copies ran while one was open for 6% of the time, Pallas kernels for 0%

profile of v1, /device:TPU:0, one launch (start us, length us, event | category | flops | bytes accessed | tf_op | source)
XLA Modules:
  0.0 348.7 jit_solution(7149659562116120236)
XLA Ops:
  0.7 1.1 fusion.8
  1.7 0.9 fusion.46
  2.6 45.3 %all-gather = bf16[16,4,4096]{2,1,0:T(4,128)(2,1)S(1)} all-gather(bf16[1,4,4096]{2,1,0:T(4,128)(2,1)S(1)} %fusion.46), channel_id=1, replica_groups=mesh['ep'=16,'tp'=2] {'ep'}, dimensions={0}, use_global_device_ids=true | all-gather | bytes 557056 | tf_op jit(solution)/shard_map/all_gather | solution.py:50
  48.0 1.3 convolution_convert_fusion.4
  49.5 0.1 copy.119
  49.6 0.7 reshape.151
  50.3 3.5 all-to-all-start.1
  53.8 0.8 fusion.10
  54.6 1.3 convolution_convert_fusion.5
  56.0 1.7 convolution_convert_fusion.3
  57.7 1.7 convolution_convert_fusion.2
  59.4 0.9 fusion.28
  60.3 1.0 subtract_exponential_fusion.1
  61.5 0.7 reshape.147
  62.5 0.7 reshape.149
  63.4 0.7 reshape.153
  64.1 6.9 %all-to-all-start = ((bf16[16,2,128]{2,1,0:T(2,128)(2,1)}), bf16[16,2,128]{2,1,0:T(2,128)(2,1)S(1)}, u32[]{:S(2)}, u32[]{:S(2)}) async-start(bf16[16,2,128]{2,1,0:T(2,128)(2,1)} %reshape.147), calls=%async_computation | async-start | bytes 16384 | tf_op jit(solution)/shard_map/all_to_all | solution.py:68
  71.3 7.0 %all-to-all-done = bf16[16,2,128]{2,1,0:T(2,128)(2,1)S(1)} async-done(((bf16[16,2,128]{2,1,0:T(2,128)(2,1)}), bf16[16,2,128]{2,1,0:T(2,128)(2,1)S(1)}, u32[]{:S(2)}, u32[]{:S(2)}) %all-to-all-start) | async-done | bytes 8224 | tf_op jit(solution)/shard_map/all_to_all | solution.py:68
  78.2 3.5 %all-to-all-start.2 = ((bf16[16,2,256]{2,1,0:T(2,128)(2,1)}), bf16[16,2,256]{2,1,0:T(2,128)(2,1)S(1)}, u32[]{:S(2)}, u32[]{:S(2)}) async-start(bf16[16,2,256]{2,1,0:T(2,128)(2,1)} %reshape.149), calls=%async_computation.2 | async-start | bytes 32768 | tf_op jit(solution)/shard_map/all_to_all | solution.py:70
  82.2 0.7 multiply_reduce_fusion.1
  83.0 6.1 %all-to-all-done.2 = bf16[16,2,256]{2,1,0:T(2,128)(2,1)S(1)} async-done(((bf16[16,2,256]{2,1,0:T(2,128)(2,1)}), bf16[16,2,256]{2,1,0:T(2,128)(2,1)S(1)}, u32[]{:S(2)}, u32[]{:S(2)}) %all-to-all-start.2) | async-done | bytes 16416 | tf_op jit(solution)/shard_map/all_to_all | solution.py:70
  89.1 3.4 all-to-all-start.3
  92.8 4.2 %multiply_add_fusion = f32[4,4,256,512]{3,2,1,0:T(8,128)S(1)} fusion(f32[4,4,256,512]{3,2,1,0:T(8,128)} %param.20, f32[4,4,512]{2,1,0:T(4,128)S(1)} %reshape.121, f32[4,4,256]{2,1,0:T(4,128)S(1)} %reshape.120, f32[4,4]{1,0:T(4,128)S(1)} %subtract_exponential_fusion, f32[4,4]{1,0:T(4,128)S(1)} %get-tuple-element.6), kind=kLoop, calls=%fused_computation | loop fusion | flops 8388608 | bytes 16826496 | tf_op jit(solution)/shard_map/add | solution.py:81
  97.0 3.4 copy-done.1
  100.4 4.0 %fusion.29 = f32[4,4,1,512]{3,2,1,0:T(1,128)S(1)} fusion(f32[4,4,256,1]{2,3,1,0:T(1,128)S(1)} %reshape.139, f32[4,4,256,512]{3,2,1,0:T(8,128)S(1)} %multiply_add_fusion), kind=kOutput, calls=%fused_computation.54 | convolution fusion | flops 25165824 | bytes 8437760 | tf_op jit(solution)/shard_map/shd,shde->she/dot_general | solution.py:85
  105.1 42.3 %all-gather.1 = bf16[16,4,2048]{2,1,0:T(4,128)(2,1)S(1)} all-gather(bf16[1,4,2048]{2,1,0:T(4,128)(2,1)S(1)} %fusion.21), channel_id=1, replica_groups=mesh['ep'=16,'tp'=2] {'ep'}, dimensions={0}, use_global_device_ids=true | all-gather | bytes 278528 | tf_op jit(solution)/shard_map/all_gather | solution.py:92
  147.4 0.8 reshape.135
  148.2 1.2 convolution_convert_fusion.1
  149.5 3.4 psum.7
  152.9 10.0 %all_to_all.65 = bf16[16,4,256]{2,1,0:T(4,128)(2,1)S(1)} all-to-all(bf16[16,4,256]{2,1,0:T(4,128)(2,1)S(1)} %psum.7), channel_id=1, replica_groups=mesh['ep'=16,'tp'=2] {'ep'}, dimensions={0} | all-to-all | bytes 65536 | tf_op jit(solution)/shard_map/all_to_all | solution.py:94
  162.9 0.1 multiply_reduce_fusion
  163.1 0.7 collective-permute-start
  163.9 6.8 %collective-permute-done = bf16[4,4096]{1,0:T(4,128)(2,1)S(1)} collective-permute-done((bf16[4,4096]{1,0:T(4,128)(2,1)S(1)}, bf16[4,4096]{1,0:T(4,128)(2,1)S(1)}, u32[]{:S(2)}, u32[]{:S(2)}) %collective-permute-start) | collective-permute-done | bytes 32800 | tf_op jit(solution)/shard_map/ppermute | solution.py:101
  170.7 7.5 %collective-permute-done.1 = bf16[4,4096]{1,0:T(4,128)(2,1)S(1)} collective-permute-done((bf16[4,4096]{1,0:T(4,128)(2,1)S(1)}, bf16[4,4096]{1,0:T(4,128)(2,1)S(1)}, u32[]{:S(2)}, u32[]{:S(2)}) %collective-permute-start.1) | collective-permute-done | bytes 32800 | tf_op jit(solution)/shard_map/ppermute | solution.py:101
  178.2 7.5 %collective-permute-done.2 = bf16[4,4096]{1,0:T(4,128)(2,1)S(1)} collective-permute-done((bf16[4,4096]{1,0:T(4,128)(2,1)S(1)}, bf16[4,4096]{1,0:T(4,128)(2,1)S(1)}, u32[]{:S(2)}, u32[]{:S(2)}) %collective-permute-start.2) | collective-permute-done | bytes 32800 | tf_op jit(solution)/shard_map/ppermute | solution.py:101
  185.7 7.5 %collective-permute-done.3 = bf16[4,4096]{1,0:T(4,128)(2,1)S(1)} collective-permute-done((bf16[4,4096]{1,0:T(4,128)(2,1)S(1)}, bf16[4,4096]{1,0:T(4,128)(2,1)S(1)}, u32[]{:S(2)}, u32[]{:S(2)}) %collective-permute-start.3) | collective-permute-done | bytes 32800 | tf_op jit(solution)/shard_map/ppermute | solution.py:101
  193.2 7.8 %collective-permute-done.4 = bf16[4,4096]{1,0:T(4,128)(2,1)S(1)} collective-permute-done((bf16[4,4096]{1,0:T(4,128)(2,1)S(1)}, bf16[4,4096]{1,0:T(4,128)(2,1)S(1)}, u32[]{:S(2)}, u32[]{:S(2)}) %collective-permute-start.4) | collective-permute-done | bytes 32800 | tf_op jit(solution)/shard_map/ppermute | solution.py:101
  201.1 7.5 %collective-permute-done.5 = bf16[4,4096]{1,0:T(4,128)(2,1)S(1)} collective-permute-done((bf16[4,4096]{1,0:T(4,128)(2,1)S(1)}, bf16[4,4096]{1,0:T(4,128)(2,1)S(1)}, u32[]{:S(2)}, u32[]{:S(2)}) %collective-permute-start.5) | collective-permute-done | bytes 32800 | tf_op jit(solution)/shard_map/ppermute | solution.py:101
  208.6 7.5 %collective-permute-done.6 = bf16[4,4096]{1,0:T(4,128)(2,1)S(1)} collective-permute-done((bf16[4,4096]{1,0:T(4,128)(2,1)S(1)}, bf16[4,4096]{1,0:T(4,128)(2,1)S(1)}, u32[]{:S(2)}, u32[]{:S(2)}) %collective-permute-start.6) | collective-permute-done | bytes 32800 | tf_op jit(solution)/shard_map/ppermute | solution.py:101
  216.1 7.5 %collective-permute-done.7 = bf16[4,4096]{1,0:T(4,128)(2,1)S(1)} collective-permute-done((bf16[4,4096]{1,0:T(4,128)(2,1)S(1)}, bf16[4,4096]{1,0:T(4,128)(2,1)S(1)}, u32[]{:S(2)}, u32[]{:S(2)}) %collective-permute-start.7) | collective-permute-done | bytes 32800 | tf_op jit(solution)/shard_map/ppermute | solution.py:101
  223.6 7.5 %collective-permute-done.8 = bf16[4,4096]{1,0:T(4,128)(2,1)S(1)} collective-permute-done((bf16[4,4096]{1,0:T(4,128)(2,1)S(1)}, bf16[4,4096]{1,0:T(4,128)(2,1)S(1)}, u32[]{:S(2)}, u32[]{:S(2)}) %collective-permute-start.8) | collective-permute-done | bytes 32800 | tf_op jit(solution)/shard_map/ppermute | solution.py:101
  231.1 0.6 copy-done.4
  231.7 7.5 %collective-permute-done.9 = bf16[4,4096]{1,0:T(4,128)(2,1)S(1)} collective-permute-done((bf16[4,4096]{1,0:T(4,128)(2,1)S(1)}, bf16[4,4096]{1,0:T(4,128)(2,1)S(1)}, u32[]{:S(2)}, u32[]{:S(2)}) %collective-permute-start.9) | collective-permute-done | bytes 32800 | tf_op jit(solution)/shard_map/ppermute | solution.py:101
  239.2 0.6 copy-done.5
  239.8 7.5 %collective-permute-done.10 = bf16[4,4096]{1,0:T(4,128)(2,1)S(1)} collective-permute-done((bf16[4,4096]{1,0:T(4,128)(2,1)S(1)}, bf16[4,4096]{1,0:T(4,128)(2,1)S(1)}, u32[]{:S(2)}, u32[]{:S(2)}) %collective-permute-start.10) | collective-permute-done | bytes 32800 | tf_op jit(solution)/shard_map/ppermute | solution.py:101
  247.3 0.6 copy-done.6
  247.9 7.5 %collective-permute-done.11 = bf16[4,4096]{1,0:T(4,128)(2,1)S(1)} collective-permute-done((bf16[4,4096]{1,0:T(4,128)(2,1)S(1)}, bf16[4,4096]{1,0:T(4,128)(2,1)S(1)}, u32[]{:S(2)}, u32[]{:S(2)}) %collective-permute-start.11) | collective-permute-done | bytes 32800 | tf_op jit(solution)/shard_map/ppermute | solution.py:101
  255.5 0.6 copy-done.7
  256.1 7.5 %collective-permute-done.12 = bf16[4,4096]{1,0:T(4,128)(2,1)S(1)} collective-permute-done((bf16[4,4096]{1,0:T(4,128)(2,1)S(1)}, bf16[4,4096]{1,0:T(4,128)(2,1)S(1)}, u32[]{:S(2)}, u32[]{:S(2)}) %collective-permute-start.12) | collective-permute-done | bytes 32800 | tf_op jit(solution)/shard_map/ppermute | solution.py:101
  263.7 0.7 copy.131
  264.3 7.0 %all-to-all-start.5 = ((f32[4,16,1]{0,2,1:T(1,128)}), f32[4,16,1]{0,2,1:T(1,128)S(1)}, u32[]{:S(2)}, u32[]{:S(2)}) async-start(f32[4,16,1]{0,2,1:T(1,128)} %copy.131), calls=%async_computation.5 | async-start | bytes 16384 | tf_op jit(solution)/shard_map/all_to_all | solution.py:114
  271.4 2.1 collective-permute-start.14
  273.5 5.1 %all-to-all-done.5 = f32[4,16,1]{0,2,1:T(1,128)S(1)} async-done(((f32[4,16,1]{0,2,1:T(1,128)}), f32[4,16,1]{0,2,1:T(1,128)S(1)}, u32[]{:S(2)}, u32[]{:S(2)}) %all-to-all-start.5) | async-done | bytes 288 | tf_op jit(solution)/shard_map/all_to_all | solution.py:114
  278.8 0.5 collective-permute-done.14
  279.2 7.1 %concatenate.8 = bf16[128,4096]{1,0:T(8,128)(2,1)S(1)} concatenate(bf16[4,4096]{1,0:T(4,128)(2,1)} %collective-permute-done.14, bf16[4,4096]{1,0:T(4,128)(2,1)} %copy-done.9, bf16[4,4096]{1,0:T(4,128)(2,1)} %copy-done.8, bf16[4,4096]{1,0:T(4,128)(2,1)} %copy-done.7, bf16[4,4096]{1,0:T(4,128)(2,1)} %copy-done.6, bf16[4,4096]{1,0:T(4,128)(2,1)} %copy-done.5, ...), dimensions={0} | concatenate | bytes 2097152 | tf_op jit(solution)/shard_map/jit(_roll_dynamic)/concatenate | solution.py:102
  286.4 2.0 fusion.1
  288.4 3.8 %convolution_convert_fusion = bf16[64,4096]{1,0:T(8,128)(2,1)} fusion(bf16[1,256,4096]{2,1,0:T(8,128)(2,1)S(1)} %copy-done, f32[64,256]{1,0:T(8,128)S(1)} %fusion.1, bf16[1,4096,256]{2,1,0:T(8,128)(2,1)} %param.33, bf16[128,4096]{1,0:T(8,128)(2,1)S(1)} %concatenate.8, s32[]{:T(128)S(6)} %select_n.24), kind=kOutput, calls=%fused_computation.1 | convolution fusion | flops 268795904 | bytes 5308420 | tf_op jit(solution)/shard_map/dot_general | solution.py:12
  292.2 1.2 convert_multiply_fusion
  293.4 1.9 reshape.118
  295.3 1.9 copy.132
  297.2 1.3 reshape.119
  298.6 47.6 %all-reduce.2 = bf16[128,2048]{1,0:T(8,128)(2,1)S(1)} all-reduce(f32[128,2048]{1,0:T(8,128)} %reshape.119), channel_id=2, replica_groups=mesh['ep'=16,'tp'=2] {'ep','tp'}, use_global_device_ids=true, to_apply=%region_5.6.clone | all-reduce | flops 262144 | bytes 1572864
  346.2 1.8 all_gather.11
  348.1 0.6 add_convert_fusion
  (86 shorter events, 2.9 us)
Async XLA Ops:
  0.6 287.8 %copy-start = (bf16[1,256,4096]{2,1,0:T(8,128)(2,1)S(1)}, bf16[1,256,4096]{2,1,0:T(8,128)(2,1)}, u32[]{:S(2)}) copy-start(bf16[1,256,4096]{2,1,0:T(8,128)(2,1)} %param.35) | copy-start | bytes 6291460
  0.6 81.5 %copy-start.11 = (f32[4,4,256]{2,1,0:T(4,128)S(1)}, f32[4,4,256]{2,1,0:T(4,128)}, u32[]{:S(2)}) copy-start(f32[4,4,256]{2,1,0:T(4,128)} %param.21) | copy-start | bytes 49156
  50.3 13.8 %all-to-all-start.1 = ((bf16[16,2,128]{2,1,0:T(2,128)(2,1)}), bf16[16,2,128]{2,1,0:T(2,128)(2,1)S(1)}, u32[]{:S(2)}, u32[]{:S(2)}) async-start(bf16[16,2,128]{2,1,0:T(2,128)(2,1)} %reshape.151), calls=%async_computation.1 | async-start | bytes 16384 | tf_op jit(solution)/shard_map/all_to_all | solution.py:69
  61.3 35.7 %copy-start.12 = (f32[4,4]{1,0:T(4,128)}, f32[4,4]{1,0:T(4,128)S(1)}, u32[]{:S(2)}) copy-start(f32[4,4]{1,0:T(4,128)S(1)} %get-tuple-element.7) | copy-start | bytes 196
  64.1 14.1 %all-to-all-start = ((bf16[16,2,128]{2,1,0:T(2,128)(2,1)}), bf16[16,2,128]{2,1,0:T(2,128)(2,1)S(1)}, u32[]{:S(2)}, u32[]{:S(2)}) async-start(bf16[16,2,128]{2,1,0:T(2,128)(2,1)} %reshape.147), calls=%async_computation | async-start | bytes 16384 | tf_op jit(solution)/shard_map/all_to_all | solution.py:68
  78.2 10.8 %all-to-all-start.2 = ((bf16[16,2,256]{2,1,0:T(2,128)(2,1)}), bf16[16,2,256]{2,1,0:T(2,128)(2,1)S(1)}, u32[]{:S(2)}, u32[]{:S(2)}) async-start(bf16[16,2,256]{2,1,0:T(2,128)(2,1)} %reshape.149), calls=%async_computation.2 | async-start | bytes 32768 | tf_op jit(solution)/shard_map/all_to_all | solution.py:70
  89.1 15.5 %all-to-all-start.3 = ((bf16[16,2,256]{2,1,0:T(2,128)(2,1)}), bf16[16,2,256]{2,1,0:T(2,128)(2,1)S(1)}, u32[]{:S(2)}, u32[]{:S(2)}) async-start(bf16[16,2,256]{2,1,0:T(2,128)(2,1)} %reshape.153), calls=%async_computation.3 | async-start | bytes 32768 | tf_op jit(solution)/shard_map/all_to_all | solution.py:71
  97.0 3.4 copy-start.1
  100.4 47.8 %copy-start.3 = (bf16[2048,256]{1,0:T(8,128)(2,1)S(1)}, bf16[2048,256]{1,0:T(8,128)(2,1)}, u32[]{:S(2)}) copy-start(bf16[2048,256]{1,0:T(8,128)(2,1)} %param.31) | copy-start | bytes 3145732
  100.4 62.5 %copy-start.2 = (bf16[4,4096]{1,0:T(4,128)(2,1)S(1)}, bf16[4,4096]{1,0:T(4,128)(2,1)}, u32[]{:S(2)}) copy-start(bf16[4,4096]{1,0:T(4,128)(2,1)} %param.19) | copy-start | bytes 98308
  100.4 62.6 %copy-start.10 = (f32[4096]{0:T(1024)S(1)}, f32[4096]{0:T(1024)}, u32[]{:S(2)}) copy-start(f32[4096]{0:T(1024)} %param.32) | copy-start | bytes 49156
  100.4 163.2 %copy-start.13 = (f32[4,2]{0,1:T(2,128)S(1)}, f32[4,2]{0,1:T(2,128)}, u32[]{:S(2)}) copy-start(f32[4,2]{0,1:T(2,128)} %param.37) | copy-start | bytes 100
  100.4 163.2 %copy-start.14 = (s32[4,2]{0,1:T(2,128)S(1)}, s32[4,2]{0,1:T(2,128)}, u32[]{:S(2)}) copy-start(s32[4,2]{0,1:T(2,128)} %param.36) | copy-start | bytes 100
  163.1 7.6 %collective-permute-start = (bf16[4,4096]{1,0:T(4,128)(2,1)S(1)}, bf16[4,4096]{1,0:T(4,128)(2,1)S(1)}, u32[]{:S(2)}, u32[]{:S(2)}) collective-permute-start(bf16[4,4096]{1,0:T(4,128)(2,1)S(1)} %multiply_convert_fusion.1), channel_id=1, source_target_pairs={{0,2},{2,4},{4,6},{6,8},{8,10},{10,12},{12,14},{14,16},{16,18},{18... | collective-permute-start | bytes 98312 | tf_op jit(solution)/shard_map/ppermute | solution.py:101
  170.7 7.5 %collective-permute-start.1 = (bf16[4,4096]{1,0:T(4,128)(2,1)S(1)}, bf16[4,4096]{1,0:T(4,128)(2,1)S(1)}, u32[]{:S(2)}, u32[]{:S(2)}) collective-permute-start(bf16[4,4096]{1,0:T(4,128)(2,1)S(1)} %collective-permute-done), channel_id=1, source_target_pairs={{0,2},{2,4},{4,6},{6,8},{8,10},{10,12},{12,14},{14,16},{16,18},{18... | collective-permute-start | bytes 98312 | tf_op jit(solution)/shard_map/ppermute | solution.py:101
  178.2 7.5 %collective-permute-start.2 = (bf16[4,4096]{1,0:T(4,128)(2,1)S(1)}, bf16[4,4096]{1,0:T(4,128)(2,1)S(1)}, u32[]{:S(2)}, u32[]{:S(2)}) collective-permute-start(bf16[4,4096]{1,0:T(4,128)(2,1)S(1)} %collective-permute-done.1), channel_id=1, source_target_pairs={{0,2},{2,4},{4,6},{6,8},{8,10},{10,12},{12,14},{14,16},{16,18},{18... | collective-permute-start | bytes 98312 | tf_op jit(solution)/shard_map/ppermute | solution.py:101
  185.7 7.5 %collective-permute-start.3 = (bf16[4,4096]{1,0:T(4,128)(2,1)S(1)}, bf16[4,4096]{1,0:T(4,128)(2,1)S(1)}, u32[]{:S(2)}, u32[]{:S(2)}) collective-permute-start(bf16[4,4096]{1,0:T(4,128)(2,1)S(1)} %collective-permute-done.2), channel_id=1, source_target_pairs={{0,2},{2,4},{4,6},{6,8},{8,10},{10,12},{12,14},{14,16},{16,18},{18... | collective-permute-start | bytes 98312 | tf_op jit(solution)/shard_map/ppermute | solution.py:101
  193.2 7.8 %collective-permute-start.4 = (bf16[4,4096]{1,0:T(4,128)(2,1)S(1)}, bf16[4,4096]{1,0:T(4,128)(2,1)S(1)}, u32[]{:S(2)}, u32[]{:S(2)}) collective-permute-start(bf16[4,4096]{1,0:T(4,128)(2,1)S(1)} %collective-permute-done.3), channel_id=1, source_target_pairs={{0,2},{2,4},{4,6},{6,8},{8,10},{10,12},{12,14},{14,16},{16,18},{18... | collective-permute-start | bytes 98312 | tf_op jit(solution)/shard_map/ppermute | solution.py:101
  201.1 7.5 %collective-permute-start.5 = (bf16[4,4096]{1,0:T(4,128)(2,1)S(1)}, bf16[4,4096]{1,0:T(4,128)(2,1)S(1)}, u32[]{:S(2)}, u32[]{:S(2)}) collective-permute-start(bf16[4,4096]{1,0:T(4,128)(2,1)S(1)} %collective-permute-done.4), channel_id=1, source_target_pairs={{0,2},{2,4},{4,6},{6,8},{8,10},{10,12},{12,14},{14,16},{16,18},{18... | collective-permute-start | bytes 98312 | tf_op jit(solution)/shard_map/ppermute | solution.py:101
  208.6 7.5 %collective-permute-start.6 = (bf16[4,4096]{1,0:T(4,128)(2,1)S(1)}, bf16[4,4096]{1,0:T(4,128)(2,1)S(1)}, u32[]{:S(2)}, u32[]{:S(2)}) collective-permute-start(bf16[4,4096]{1,0:T(4,128)(2,1)S(1)} %collective-permute-done.5), channel_id=1, source_target_pairs={{0,2},{2,4},{4,6},{6,8},{8,10},{10,12},{12,14},{14,16},{16,18},{18... | collective-permute-start | bytes 98312 | tf_op jit(solution)/shard_map/ppermute | solution.py:101
  216.1 7.5 %collective-permute-start.7 = (bf16[4,4096]{1,0:T(4,128)(2,1)S(1)}, bf16[4,4096]{1,0:T(4,128)(2,1)S(1)}, u32[]{:S(2)}, u32[]{:S(2)}) collective-permute-start(bf16[4,4096]{1,0:T(4,128)(2,1)S(1)} %collective-permute-done.6), channel_id=1, source_target_pairs={{0,2},{2,4},{4,6},{6,8},{8,10},{10,12},{12,14},{14,16},{16,18},{18... | collective-permute-start | bytes 98312 | tf_op jit(solution)/shard_map/ppermute | solution.py:101
  223.6 7.5 %collective-permute-start.8 = (bf16[4,4096]{1,0:T(4,128)(2,1)S(1)}, bf16[4,4096]{1,0:T(4,128)(2,1)S(1)}, u32[]{:S(2)}, u32[]{:S(2)}) collective-permute-start(bf16[4,4096]{1,0:T(4,128)(2,1)S(1)} %collective-permute-done.7), channel_id=1, source_target_pairs={{0,2},{2,4},{4,6},{6,8},{8,10},{10,12},{12,14},{14,16},{16,18},{18... | collective-permute-start | bytes 98312 | tf_op jit(solution)/shard_map/ppermute | solution.py:101
  231.1 0.6 copy-start.4
  231.7 7.5 %collective-permute-start.9 = (bf16[4,4096]{1,0:T(4,128)(2,1)S(1)}, bf16[4,4096]{1,0:T(4,128)(2,1)S(1)}, u32[]{:S(2)}, u32[]{:S(2)}) collective-permute-start(bf16[4,4096]{1,0:T(4,128)(2,1)S(1)} %collective-permute-done.8), channel_id=1, source_target_pairs={{0,2},{2,4},{4,6},{6,8},{8,10},{10,12},{12,14},{14,16},{16,18},{18... | collective-permute-start | bytes 98312 | tf_op jit(solution)/shard_map/ppermute | solution.py:101
  239.2 0.6 copy-start.5
  239.8 7.5 %collective-permute-start.10 = (bf16[4,4096]{1,0:T(4,128)(2,1)S(1)}, bf16[4,4096]{1,0:T(4,128)(2,1)S(1)}, u32[]{:S(2)}, u32[]{:S(2)}) collective-permute-start(bf16[4,4096]{1,0:T(4,128)(2,1)S(1)} %collective-permute-done.9), channel_id=1, source_target_pairs={{0,2},{2,4},{4,6},{6,8},{8,10},{10,12},{12,14},{14,16},{16,18},{18... | collective-permute-start | bytes 98312 | tf_op jit(solution)/shard_map/ppermute | solution.py:101
  247.3 0.6 copy-start.6
  247.9 7.5 %collective-permute-start.11 = (bf16[4,4096]{1,0:T(4,128)(2,1)S(1)}, bf16[4,4096]{1,0:T(4,128)(2,1)S(1)}, u32[]{:S(2)}, u32[]{:S(2)}) collective-permute-start(bf16[4,4096]{1,0:T(4,128)(2,1)S(1)} %collective-permute-done.10), channel_id=1, source_target_pairs={{0,2},{2,4},{4,6},{6,8},{8,10},{10,12},{12,14},{14,16},{16,18},{18... | collective-permute-start | bytes 98312 | tf_op jit(solution)/shard_map/ppermute | solution.py:101
  255.5 0.6 copy-start.7
  256.1 7.5 %collective-permute-start.12 = (bf16[4,4096]{1,0:T(4,128)(2,1)S(1)}, bf16[4,4096]{1,0:T(4,128)(2,1)S(1)}, u32[]{:S(2)}, u32[]{:S(2)}) collective-permute-start(bf16[4,4096]{1,0:T(4,128)(2,1)S(1)} %collective-permute-done.11), channel_id=1, source_target_pairs={{0,2},{2,4},{4,6},{6,8},{8,10},{10,12},{12,14},{14,16},{16,18},{18... | collective-permute-start | bytes 98312 | tf_op jit(solution)/shard_map/ppermute | solution.py:101
  263.6 15.2 %copy-start.8 = (bf16[4,4096]{1,0:T(4,128)(2,1)}, bf16[4,4096]{1,0:T(4,128)(2,1)S(1)}, u32[]{:S(2)}) copy-start(bf16[4,4096]{1,0:T(4,128)(2,1)S(1)} %collective-permute-done.12) | copy-start | bytes 98308
  263.6 7.8 %collective-permute-start.13 = (bf16[4,4096]{1,0:T(4,128)(2,1)S(1)}, bf16[4,4096]{1,0:T(4,128)(2,1)S(1)}, u32[]{:S(2)}, u32[]{:S(2)}) collective-permute-start(bf16[4,4096]{1,0:T(4,128)(2,1)S(1)} %collective-permute-done.12), channel_id=1, source_target_pairs={{0,2},{2,4},{4,6},{6,8},{8,10},{10,12},{12,14},{14,16},{16,18},{18... | collective-permute-start | bytes 98312 | tf_op jit(solution)/shard_map/ppermute | solution.py:101
  264.3 14.3 %all-to-all-start.5 = ((f32[4,16,1]{0,2,1:T(1,128)}), f32[4,16,1]{0,2,1:T(1,128)S(1)}, u32[]{:S(2)}, u32[]{:S(2)}) async-start(f32[4,16,1]{0,2,1:T(1,128)} %copy.131), calls=%async_computation.5 | async-start | bytes 16384 | tf_op jit(solution)/shard_map/all_to_all | solution.py:114
  271.4 7.4 %copy-start.9 = (bf16[4,4096]{1,0:T(4,128)(2,1)}, bf16[4,4096]{1,0:T(4,128)(2,1)S(1)}, u32[]{:S(2)}) copy-start(bf16[4,4096]{1,0:T(4,128)(2,1)S(1)} %collective-permute-done.13) | copy-start | bytes 98308
  271.4 7.8 %collective-permute-start.14 = (bf16[4,4096]{1,0:T(4,128)(2,1)S(1)}, bf16[4,4096]{1,0:T(4,128)(2,1)}, u32[]{:S(2)}, u32[]{:S(2)}) collective-permute-start(bf16[4,4096]{1,0:T(4,128)(2,1)S(1)} %collective-permute-done.13), channel_id=1, source_target_pairs={{0,2},{2,4},{4,6},{6,8},{8,10},{10,12},{12,14},{14,16},{16,18},{18... | collective-permute-start | bytes 98312 | tf_op jit(solution)/shard_map/ppermute | solution.py:101
